TPU v7x, 32 devices: a whole 2x2x4 slice. The times are simulated.
32 devices in a mesh: ep: 8 (over z, x), tp: 4 (over y, core).
Axes of the slice: x: 2, y: 2, z: 4, core: 2. Of those that a mesh axis runs over, the one named last changes fastest.
Arguments:
- tokens: bfloat16 [4096, 4096], P('ep', 'tp'), may hold values from -100 to 100, as said below
- routes: int32 [4096, 2], P('ep'), may hold values from 0 to 15, all different within a row; in each aligned block of 512 rows (0 to 511, 512 to 1023, ...) at most 128 rows name the same one
- route_weights: float32 [4096, 2], P('ep'), may hold values from 0.1 to 1
- norm_gain: float32 [4096], P('tp'), may hold values from 0.1 to 1.9
- gate_weight: bfloat16 [16, 4096, 512], P('ep', 'tp'), may hold values from -0.09375 to 0.09375
- up_weight: bfloat16 [16, 4096, 512], P('ep', 'tp'), may hold values from -0.09375 to 0.09375
- down_weight: bfloat16 [16, 512, 4096], P('ep', None, 'tp'), may hold values from -0.25 to 0.25
- final_gain: float32 [4096], P('tp'), may hold values from 0.1 to 1.9
Outputs:
- mixed: bfloat16 [4096, 4096], P('ep', 'tp')
Inputs may be any that keep to these rules, and one draw needn't show every extreme that they name: `tokens`: real-valued activations whose features differ in scale. `routes`: each row names 2 different experts; among the 512 rows of one aligned block no expert is named more than 128 times, a bound that some block reaches.
All inputs are finite; a program needn't handle non-finite values.
Results may differ from a plain program's by a relative error of at most 0.018.
Values may be sent and summed in bfloat16 or wider, within the bound.
A program may use at most 64 MiB of HBM per device.

v0:
```python
import jax
import jax.numpy as jnp
from jax import lax
from jax.sharding import PartitionSpec as P

D = 4096
EPSILON = 1e-06


def expert_rows(weights, block):
    w_gate, w_up, w_down = weights
    gate = jnp.einsum("scd,df->scf", block, w_gate, preferred_element_type=jnp.float32)
    upper = jnp.einsum("scd,df->scf", block, w_up, preferred_element_type=jnp.float32)
    gate_sum, upper_sum = (
        lax.psum_scatter(gate.astype(jnp.bfloat16), "tp", scatter_dimension=2, tiled=True).astype(
            jnp.float32
        ),
        lax.psum_scatter(upper.astype(jnp.bfloat16), "tp", scatter_dimension=2, tiled=True).astype(
            jnp.float32
        ),
    )
    share = (jax.nn.silu(gate_sum) * upper_sum).astype(jnp.bfloat16)
    hidden = lax.all_gather(share, "tp", axis=2, tiled=True)
    return jnp.einsum("scf,fd->scd", hidden, w_down, preferred_element_type=jnp.float32).astype(
        jnp.bfloat16
    )


def serve_single(weights, block):
    return lax.all_to_all(
        expert_rows(weights, block), "ep", split_axis=0, concat_axis=0, tiled=True
    )


def body(tokens, routes, route_weights, norm_gain, gate_weight, up_weight, down_weight, final_gain):
    ep_count = lax.axis_size("ep")
    local_count = gate_weight.shape[0]
    experts = ep_count * local_count
    tok_rows = tokens.shape[0]
    top_count = routes.shape[1]
    capacity = 4 * tok_rows // experts
    values = tokens.astype(jnp.float32)
    squares = lax.psum(jnp.sum(values * values, axis=-1), "tp")
    normed = (values * lax.rsqrt(squares / D + EPSILON)[:, None] * norm_gain).astype(jnp.bfloat16)
    chosen = routes.reshape(-1)
    onehot = (chosen[:, None] == jnp.arange(experts, dtype=jnp.int32)[None, :]).astype(jnp.int32)
    slots = jnp.sum((jnp.cumsum(onehot, axis=0) - onehot) * onehot, axis=1)
    target = chosen * capacity + slots
    owners = jnp.arange(tok_rows * top_count, dtype=jnp.int32) // top_count
    table = jnp.full((experts * capacity,), tok_rows, jnp.int32).at[target].set(owners)
    padded = jnp.concatenate([normed, jnp.zeros((1, normed.shape[1]), jnp.bfloat16)], axis=0)
    outgoing = padded[table].reshape(ep_count, local_count, capacity, normed.shape[1])
    weight_list = [
        (gate_weight[member], up_weight[member], down_weight[member])
        for member in range(local_count)
    ]
    pieces = []
    for member in range(local_count):
        pieces.append(
            serve_single(
                weight_list[member],
                lax.all_to_all(outgoing[:, member], "ep", split_axis=0, concat_axis=0, tiled=True),
            )
        )
    arrived = jnp.stack(pieces, axis=1)
    returned = arrived.reshape(experts * capacity, normed.shape[1])
    position = target.reshape(tok_rows, top_count)
    combined = jnp.zeros((tok_rows, normed.shape[1]), jnp.float32)
    for which in range(top_count):
        combined = combined + route_weights[:, which : which + 1] * returned[
            position[:, which]
        ].astype(jnp.float32)
    closing = lax.psum(jnp.sum(combined * combined, axis=-1), "tp")
    return (combined * lax.rsqrt(closing / D + EPSILON)[:, None] * final_gain).astype(jnp.bfloat16)


def solution(mesh):
    in_specs = (
        P("ep", "tp"),
        P("ep", None),
        P("ep", None),
        P("tp"),
        P("ep", "tp", None),
        P("ep", "tp", None),
        P("ep", None, "tp"),
        P("tp"),
    )
    out_specs = P("ep", "tp")
    return jax.shard_map(body, mesh=mesh, in_specs=in_specs, out_specs=out_specs, check_vma=False)
```

profile of v0, /device:TPU:0, one launch (start us, length us, event | category | flops | bytes accessed | tf_op | source)
XLA Modules:
  0.0 332.4 jit_solution(4399818030590045528)
XLA Ops:
  7.8 1.5 fusion
  9.3 8.4 %psum.14 = f32[512]{0:T(512)S(1)} all-reduce(f32[512]{0:T(512)S(1)} %fusion), channel_id=1, replica_groups=mesh['ep'=8,'tp'=4] {'tp'}, use_global_device_ids=true, to_apply=%region_1.0 | all-reduce | flops 512 | bytes 4096 | tf_op jit(solution)/shard_map/psum | solution.py:43
  17.7 4.5 %reduce-window.6 = s32[16,8,128]{2,1,0:T(8,128)S(1)} reduce-window(s32[16,8,128]{2,1,0:T(8,128)S(1)} %fusion.30, s32[]{:T(128)} %constant.41.clone.1), window={size=1x1x128 pad=0_0x0_0x127_0}, to_apply=%region_2.0 | reduce-window | flops 2080768 | bytes 131076 | tf_op jit(solution)/shard_map/reduce-window
  23.1 4.3 %scatter_custom_fusion = s32[2048]{0:T(1024)S(1)} fusion(s32[1024]{0:T(1024)S(1)} %bitcast.128, s32[1024]{0:T(1024)S(1)} %add_select_fusion, s32[]{:T(128)} %constant.39.clone.1), kind=kCustom, calls=%fused_computation.75 | custom fusion | bytes 8196 | tf_op jit(solution)/shard_map/scatter | solution.py:50
  27.9 9.7 %gather_fusion = bf16[2048,1024]{1,0:T(8,128)(2,1)} fusion(bf16[513,1024]{1,0:T(8,128)(2,1)S(1)} %concatenate.3, s32[2048]{0:T(1024)S(1)} %fusion.31), kind=kCustom, calls=%fused_computation | custom fusion | bytes 8396800 | tf_op jit(solution)/shard_map/gather | solution.py:52
  37.6 4.0 %slice_bitcast_fusion.1 = (bf16[8,128,1024]{2,1,0:T(8,128)(2,1)}, bf16[8,128,1024]{2,1,0:T(8,128)(2,1)S(1)}) fusion(bf16[8,2,128,1024]{3,2,1,0:T(8,128)(2,1)} %bitcast.103), kind=kLoop, calls=%fused_computation.11 | loop fusion | bytes 8388608 | tf_op jit(solution)/shard_map/squeeze | solution.py:62
  41.7 52.7 %all_to_all.20 = bf16[8,128,1024]{2,1,0:T(8,128)(2,1)S(1)} all-to-all(bf16[8,128,1024]{2,1,0:T(8,128)(2,1)S(1)} %get-tuple-element.8), channel_id=1, replica_groups=mesh['ep'=8,'tp'=4] {'ep'}, dimensions={0} | all-to-all | bytes 4194304 | tf_op jit(solution)/shard_map/all_to_all | solution.py:62
  94.4 2.2 convolution_convert_fusion.2
  96.6 1.7 copy.41
  99.6 4.4 %all-to-all-start = ((bf16[8,128,1024]{2,1,0:T(8,128)(2,1)}), bf16[8,128,1024]{2,1,0:T(8,128)(2,1)}, u32[]{:S(2)}, u32[]{:S(2)}) async-start(bf16[8,128,1024]{2,1,0:T(8,128)(2,1)} %get-tuple-element.7), calls=%async_computation | async-start | bytes 4194304 | tf_op jit(solution)/shard_map/all_to_all | solution.py:62
  104.0 3.4 %convolution_convert_fusion.3 = bf16[8,128,512]{2,1,0:T(8,128)(2,1)} fusion(bf16[8,128,1024]{2,1,0:T(8,128)(2,1)S(1)} %all_to_all.20, bf16[2,1024,512]{2,1,0:T(8,128)(2,1)} %param.12), kind=kOutput, calls=%fused_computation.18 | convolution fusion | flops 1074266112 | bytes 4194304 | tf_op jit(solution)/shard_map/scd,df->scf/dot_general | solution.py:12
  107.5 1.7 copy.39
  110.5 13.1 %reduce-scatter.19.cloned.1.call-done = bf16[128,1024]{1,0:T(8,128)(2,1)} async-done(((bf16[512,1024]{1,0:T(8,128)(2,1)}), bf16[128,1024]{1,0:T(8,128)(2,1)}) %reduce-scatter.19.cloned.1.call-update) | async-done | bytes 262160
  124.9 26.1 %reduce-scatter.17.cloned.1.call-done = bf16[128,1024]{1,0:T(8,128)(2,1)} async-done(((bf16[512,1024]{1,0:T(8,128)(2,1)}), bf16[128,1024]{1,0:T(8,128)(2,1)}) %reduce-scatter.17.cloned.1.call-update) | async-done | bytes 262160
  153.2 3.1 convolution_convert_fusion.4
  158.4 3.2 convolution_convert_fusion.5
  162.4 1.3 copy.62
  163.7 6.5 %all-gather.5.cloned.1.call-done = bf16[8,128,512]{2,1,0:T(8,128)(2,1)} async-done(((bf16[8,128,128]{2,1,0:T(8,128)(2,1)}), bf16[8,128,512]{2,1,0:T(8,128)(2,1)}) %all-gather.5.cloned.1.call-update) | async-done | bytes 1048592 | tf_op jit(solution)/shard_map/all_gather | solution.py:23
  170.1 3.8 %convolution_convert_fusion = bf16[8,128,1024]{2,1,0:T(8,128)(2,1)} fusion(bf16[8,128,512]{2,1,0:T(8,128)(2,1)} %all-gather.5.cloned.1.call-done, bf16[2,512,1024]{2,1,0:T(8,128)(2,1)S(1)} %copy-done.5), kind=kOutput, calls=%fused_computation.15 | convolution fusion | flops 1074790400 | bytes 4194304 | tf_op jit(solution)/shard_map/scf,fd->scd/dot_general | solution.py:24
  174.0 5.5 %all-to-all-start.3 = ((bf16[8,128,1024]{2,1,0:T(8,128)(2,1)}), bf16[8,128,1024]{2,1,0:T(8,128)(2,1)S(1)}, u32[]{:S(2)}, u32[]{:S(2)}) async-start(bf16[8,128,1024]{2,1,0:T(8,128)(2,1)} %convolution_convert_fusion), calls=%async_computation.3 | async-start | bytes 4194304 | tf_op jit(solution)/shard_map/all_to_all | solution.py:30
  179.7 17.6 %reduce-scatter.15.cloned.1.call-done = bf16[128,1024]{1,0:T(8,128)(2,1)} async-done(((bf16[512,1024]{1,0:T(8,128)(2,1)}), bf16[128,1024]{1,0:T(8,128)(2,1)}) %reduce-scatter.15.cloned.1.call-update) | async-done | bytes 262160
  198.6 26.0 %reduce-scatter.13.cloned.1.call-done = bf16[128,1024]{1,0:T(8,128)(2,1)} async-done(((bf16[512,1024]{1,0:T(8,128)(2,1)}), bf16[128,1024]{1,0:T(8,128)(2,1)}) %reduce-scatter.13.cloned.1.call-update) | async-done | bytes 262160
  226.7 17.0 %all-gather.3.cloned.1.call-done = bf16[8,128,512]{2,1,0:T(8,128)(2,1)} async-done(((bf16[8,128,128]{2,1,0:T(8,128)(2,1)}), bf16[8,128,512]{2,1,0:T(8,128)(2,1)}) %all-gather.3.cloned.1.call-update) | async-done | bytes 1048592 | tf_op jit(solution)/shard_map/all_gather | solution.py:23
  243.6 4.1 %convolution_convert_fusion.1 = bf16[8,128,1024]{2,1,0:T(8,128)(2,1)} fusion(bf16[8,128,512]{2,1,0:T(8,128)(2,1)} %all-gather.3.cloned.1.call-done, bf16[2,512,1024]{2,1,0:T(8,128)(2,1)} %param.14), kind=kOutput, calls=%fused_computation.16 | convolution fusion | flops 1074790400 | bytes 4194304 | tf_op jit(solution)/shard_map/scf,fd->scd/dot_general | solution.py:24
  247.7 5.6 %all-to-all-start.1 = ((bf16[8,128,1024]{2,1,0:T(8,128)(2,1)}), bf16[8,128,1024]{2,1,0:T(8,128)(2,1)}, u32[]{:S(2)}, u32[]{:S(2)}) async-start(bf16[8,128,1024]{2,1,0:T(8,128)(2,1)} %convolution_convert_fusion.1), calls=%async_computation.1 | async-start | bytes 4194304 | tf_op jit(solution)/shard_map/all_to_all | solution.py:30
  253.7 48.4 %all-to-all-done.1 = bf16[8,128,1024]{2,1,0:T(8,128)(2,1)} async-done(((bf16[8,128,1024]{2,1,0:T(8,128)(2,1)}), bf16[8,128,1024]{2,1,0:T(8,128)(2,1)}, u32[]{:S(2)}, u32[]{:S(2)}) %all-to-all-start.1) | async-done | bytes 2097184 | tf_op jit(solution)/shard_map/all_to_all | solution.py:30
  302.1 2.0 pad_maximum_fusion
  304.1 2.4 copy.34
  306.5 5.5 %gather_fusion.2 = bf16[512,1024]{1,0:T(8,128)(2,1)S(1)} fusion(bf16[2048,1024]{1,0:T(8,128)(2,1)} %bitcast.101, s32[1024]{0:T(1024)S(1)} %get-tuple-element.13), kind=kCustom, calls=%fused_computation.2 | custom fusion | bytes 2099200 | tf_op jit(solution)/shard_map/gather | solution.py:70
  311.9 5.5 %gather_fusion.1 = bf16[512,1024]{1,0:T(8,128)(2,1)S(1)} fusion(bf16[2048,1024]{1,0:T(8,128)(2,1)} %bitcast.102, s32[1024]{0:T(1024)S(1)} %get-tuple-element.14), kind=kCustom, calls=%fused_computation.1 | custom fusion | bytes 2099200 | tf_op jit(solution)/shard_map/gather | solution.py:70
  318.0 5.9 %psum.15 = f32[512]{0:T(512)S(1)} all-reduce(f32[512]{0:T(512)S(1)} %multiply_reduce_fusion), channel_id=1, replica_groups=mesh['ep'=8,'tp'=4] {'tp'}, use_global_device_ids=true, to_apply=%region_11.12 | all-reduce | flops 512 | bytes 4096 | tf_op jit(solution)/shard_map/psum | solution.py:73
  324.0 1.6 multiply_convert_fusion
  (66 shorter events, 15.9 us)
Async XLA Ops:
  6.5 21.0 %copy-start = (bf16[512,1024]{1,0:T(8,128)(2,1)S(1)}, bf16[512,1024]{1,0:T(8,128)(2,1)}, u32[]{:S(2)}) copy-start(bf16[512,1024]{1,0:T(8,128)(2,1)} %param.8) | copy-start | bytes 3145732
  6.5 21.0 %copy-start.1 = (f32[1024]{0:T(1024)S(1)}, f32[1024]{0:T(1024)}, u32[]{:S(2)}) copy-start(f32[1024]{0:T(1024)} %param.11) | copy-start | bytes 12292
  6.5 117.1 %reduce-scatter.19.cloned.1.call-start = ((), (), s32[]{:S(2)}) async-start(), calls=%async_computation.13 | async-start | bytes 1310720
  41.6 52.7 %copy-start.4 = (bf16[2,1024,512]{2,1,0:T(8,128)(2,1)S(1)}, bf16[2,1024,512]{2,1,0:T(8,128)(2,1)}, u32[]{:S(2)}) copy-start(bf16[2,1024,512]{2,1,0:T(8,128)(2,1)} %param.13) | copy-start | bytes 6291460
  99.6 53.6 %all-to-all-start = ((bf16[8,128,1024]{2,1,0:T(8,128)(2,1)}), bf16[8,128,1024]{2,1,0:T(8,128)(2,1)}, u32[]{:S(2)}, u32[]{:S(2)}) async-start(bf16[8,128,1024]{2,1,0:T(8,128)(2,1)} %get-tuple-element.7), calls=%async_computation | async-start | bytes 4194304 | tf_op jit(solution)/shard_map/all_to_all | solution.py:62
  104.0 47.0 %reduce-scatter.17.cloned.1.call-start = ((), (), s32[]{:S(2)}) async-start(), calls=%async_computation.12 | async-start | bytes 1310720
  110.5 59.6 %all-gather.5.cloned.1.call-start = ((), (), s32[]{:S(2)}) async-start(), calls=%async_computation.9 | async-start | bytes 1310720 | tf_op jit(solution)/shard_map/all_gather | solution.py:23
  153.1 44.2 %reduce-scatter.15.cloned.1.call-start = ((), (), s32[]{:S(2)}) async-start(), calls=%async_computation.11 | async-start | bytes 1310720
  158.3 66.2 %reduce-scatter.13.cloned.1.call-start = ((), (), s32[]{:S(2)}) async-start(), calls=%async_computation.10 | async-start | bytes 1310720
  162.4 7.8 %copy-start.5 = (bf16[2,512,1024]{2,1,0:T(8,128)(2,1)S(1)}, bf16[2,512,1024]{2,1,0:T(8,128)(2,1)}, u32[]{:S(2)}) copy-start(bf16[2,512,1024]{2,1,0:T(8,128)(2,1)} %param.14) | copy-start | bytes 6291460
  174.0 73.8 %all-to-all-start.3 = ((bf16[8,128,1024]{2,1,0:T(8,128)(2,1)}), bf16[8,128,1024]{2,1,0:T(8,128)(2,1)S(1)}, u32[]{:S(2)}, u32[]{:S(2)}) async-start(bf16[8,128,1024]{2,1,0:T(8,128)(2,1)} %convolution_convert_fusion), calls=%async_computation.3 | async-start | bytes 4194304 | tf_op jit(solution)/shard_map/all_to_all | solution.py:30
  179.5 64.2 %all-gather.3.cloned.1.call-start = ((), (), s32[]{:S(2)}) async-start(), calls=%async_computation.8 | async-start | bytes 1310720 | tf_op jit(solution)/shard_map/all_gather | solution.py:23
  247.7 6.0 %copy-start.3 = (f32[512,2]{0,1:T(2,128)S(1)}, f32[512,2]{0,1:T(2,128)}, u32[]{:S(2)}) copy-start(f32[512,2]{0,1:T(2,128)} %param.10) | copy-start | bytes 12292
  247.7 54.4 %all-to-all-start.1 = ((bf16[8,128,1024]{2,1,0:T(8,128)(2,1)}), bf16[8,128,1024]{2,1,0:T(8,128)(2,1)}, u32[]{:S(2)}, u32[]{:S(2)}) async-start(bf16[8,128,1024]{2,1,0:T(8,128)(2,1)} %convolution_convert_fusion.1), calls=%async_computation.1 | async-start | bytes 4194304 | tf_op jit(solution)/shard_map/all_to_all | solution.py:30
  317.4 6.6 %copy-start.2 = (f32[1024]{0:T(1024)S(1)}, f32[1024]{0:T(1024)}, u32[]{:S(2)}) copy-start(f32[1024]{0:T(1024)} %param.15) | copy-start | bytes 12292
Sparse Core Ops, SparseCore 0:
  99.7 23.8 reduce-scatter.18
  126.1 24.8 reduce-scatter.16
  153.3 16.8 all-gather.4
  172.5 24.7 reduce-scatter.14
  199.7 24.7 reduce-scatter.12
  226.8 16.8 all-gather.2
where the time goes:
time: 333 us; the launch traced here: 332 us
  waiting for transfers between devices  155 us (47%)
  blocking collectives  67.1 us (20%)
  local copies, waits for them, and re-layouts  48.2 us (14%)
  matrix products  19.9 us (6%)
  starting transfers between devices  15.9 us (5%)
  between operations  13.8 us (4%)
  other arithmetic  12.8 us (4%)
    unnamed x10, waiting for transfers between devices  82.9 us
    all_to_all x1, blocking collectives, body(): lax.all_to_all(outgoing[:, member], 'ep', split_axis=0, concat_axis=0, ti...  52.7 us
    all_to_all x2, waiting for transfers between devices, serve_single(): lax.all_to_all(expert_rows(weights, block), 'ep', split_axis=0, concat_ax...  48.4 us
    all_gather x2, waiting for transfers between devices, expert_rows(): hidden = lax.all_gather(share, 'tp', axis=2, tiled=True)  23.4 us
    unnamed x29, local copies, waits for them, and re-layouts  15.8 us
    all_to_all x2, starting transfers between devices, serve_single(): lax.all_to_all(expert_rows(weights, block), 'ep', split_axis=0, concat_ax...  11.2 us
    gather x2, local copies, waits for them, and re-layouts, body(): returned[position[:, which]].astype(jnp.float32)  10.9 us
    gather x1, local copies, waits for them, and re-layouts, body(): padded[table].reshape(ep_count, local_count, capacity, normed.shape[1])  9.7 us
  transfers between devices with their start and end apart: 9, of which 7 were waited for; matrix products, arithmetic and copies ran while one was open for 10% of the time, Pallas kernels for 0%

commit v1 on v0

--- a/solution.py
+++ b/solution.py
@@ -20,7 +20,12 @@
         ),
     )
     share = (jax.nn.silu(gate_sum) * upper_sum).astype(jnp.bfloat16)
-    hidden = lax.all_gather(share, "tp", axis=2, tiled=True)
+    ring = [share]
+    for hop in range(3):
+        ring.append(lax.ppermute(ring[-1], "tp", [(dev, (dev + 1) % 4) for dev in range(4)]))
+    hidden = jnp.roll(
+        jnp.concatenate(ring[::-1], axis=2), (lax.axis_index("tp") + 1) * ring[0].shape[2], axis=2
+    )
     return jnp.einsum("scf,fd->scd", hidden, w_down, preferred_element_type=jnp.float32).astype(
         jnp.bfloat16
     )

time: 333 us -> 320 us (0.961)
  waiting for transfers between devices: 155 us -> 145 us
  starting transfers between devices: 15.9 us -> 12.5 us
    unnamed x10 -> x8, waiting for transfers between devices: 82.9 us -> 18.6 us
    all_to_all x1, waiting for transfers between devices: 0.01 us -> 40.7 us  [body(): lax.all_to_all(outgoing[:, member], 'ep', split_axis=0, concat_axis=0, ti...]
    ppermute x0 -> x6, waiting for transfers between devices: none -> 34.8 us  [expert_rows(): lax.ppermute(ring[-1], 'tp', [(dev, (dev + 1) % 4) for dev in range(4)])]
    all_gather x2 -> x0, waiting for transfers between devices: 23.4 us -> none  [expert_rows(): hidden = lax.all_gather(share, 'tp', axis=2, tiled=True)]
    unnamed x29 -> x27, local copies, waits for them, and re-layouts: 15.8 us -> 15.8 us
  transfers between devices with their start and end apart: 9 -> 13, of which waited for: 7 -> 10; matrix products, arithmetic and copies ran while one was open for 10% -> 10% of each run, Pallas kernels for 0% -> 0%
where the time goes in v1:
time: 320 us; the launch traced here: 319 us
  waiting for transfers between devices  145 us (45%)
  blocking collectives  66.8 us (21%)
  local copies, waits for them, and re-layouts  48.1 us (15%)
  matrix products  20.9 us (7%)
  between operations  13.5 us (4%)
  starting transfers between devices  12.5 us (4%)
  other arithmetic  11.4 us (4%)
    all_to_all x1, blocking collectives, body(): lax.all_to_all(outgoing[:, member], 'ep', split_axis=0, concat_axis=0, ti...  52.7 us
    all_to_all x2, waiting for transfers between devices, serve_single(): lax.all_to_all(expert_rows(weights, block), 'ep', split_axis=0, concat_ax...  51.4 us
    all_to_all x1, waiting for transfers between devices, body(): lax.all_to_all(outgoing[:, member], 'ep', split_axis=0, concat_axis=0, ti...  40.7 us
    ppermute x6, waiting for transfers between devices, expert_rows(): lax.ppermute(ring[-1], 'tp', [(dev, (dev + 1) % 4) for dev in range(4)])  34.8 us
    unnamed x8, waiting for transfers between devices  18.6 us
    unnamed x27, local copies, waits for them, and re-layouts  15.8 us
    gather x2, local copies, waits for them, and re-layouts, body(): returned[position[:, which]].astype(jnp.float32)  10.9 us
    gather x1, local copies, waits for them, and re-layouts, body(): padded[table].reshape(ep_count, local_count, capacity, normed.shape[1])  9.67 us
  transfers between devices with their start and end apart: 13, of which 10 were waited for; matrix products, arithmetic and copies ran while one was open for 10% of the time, Pallas kernels for 0%

profile of v1, /device:TPU:0, one launch (start us, length us, event | category | flops | bytes accessed | tf_op | source)
XLA Modules:
  0.0 318.7 jit_solution(8232916756196982892)
XLA Ops:
  9.3 8.4 %psum.14 = f32[512]{0:T(512)S(1)} all-reduce(f32[512]{0:T(512)S(1)} %fusion), channel_id=1, replica_groups=mesh['ep'=8,'tp'=4] {'tp'}, use_global_device_ids=true, to_apply=%region_1.0 | all-reduce | flops 512 | bytes 4096 | tf_op jit(solution)/shard_map/psum | solution.py:48
  17.7 4.5 %reduce-window.6 = s32[16,8,128]{2,1,0:T(8,128)S(1)} reduce-window(s32[16,8,128]{2,1,0:T(8,128)S(1)} %fusion.48, s32[]{:T(128)} %constant.63.clone.1), window={size=1x1x128 pad=0_0x0_0x127_0}, to_apply=%region_2.0 | reduce-window | flops 2080768 | bytes 131076 | tf_op jit(solution)/shard_map/reduce-window
  23.1 4.3 %scatter_custom_fusion = s32[2048]{0:T(1024)S(1)} fusion(s32[1024]{0:T(1024)S(1)} %bitcast.126, s32[1024]{0:T(1024)S(1)} %add_select_fusion, s32[]{:T(128)} %constant.61.clone.1), kind=kCustom, calls=%fused_computation.107 | custom fusion | bytes 8196 | tf_op jit(solution)/shard_map/scatter | solution.py:55
  27.9 9.7 %gather_fusion = bf16[2048,1024]{1,0:T(8,128)(2,1)} fusion(bf16[513,1024]{1,0:T(8,128)(2,1)S(1)} %concatenate.12, s32[2048]{0:T(1024)S(1)} %fusion.49), kind=kCustom, calls=%fused_computation | custom fusion | bytes 8396800 | tf_op jit(solution)/shard_map/gather | solution.py:57
  37.6 4.0 %slice_bitcast_fusion.1 = (bf16[8,128,1024]{2,1,0:T(8,128)(2,1)}, bf16[8,128,1024]{2,1,0:T(8,128)(2,1)S(1)}) fusion(bf16[8,2,128,1024]{3,2,1,0:T(8,128)(2,1)} %bitcast.101), kind=kLoop, calls=%fused_computation.11 | loop fusion | bytes 8388608 | tf_op jit(solution)/shard_map/squeeze | solution.py:67
  41.6 52.7 %all_to_all.20 = bf16[8,128,1024]{2,1,0:T(8,128)(2,1)S(1)} all-to-all(bf16[8,128,1024]{2,1,0:T(8,128)(2,1)S(1)} %get-tuple-element.9), channel_id=1, replica_groups=mesh['ep'=8,'tp'=4] {'ep'}, dimensions={0} | all-to-all | bytes 4194304 | tf_op jit(solution)/shard_map/all_to_all | solution.py:67
  94.3 2.2 convolution_convert_fusion.2
  96.5 1.7 copy.41
  99.5 4.4 %all-to-all-start = ((bf16[8,128,1024]{2,1,0:T(8,128)(2,1)}), bf16[8,128,1024]{2,1,0:T(8,128)(2,1)}, u32[]{:S(2)}, u32[]{:S(2)}) async-start(bf16[8,128,1024]{2,1,0:T(8,128)(2,1)} %get-tuple-element.8), calls=%async_computation | async-start | bytes 4194304 | tf_op jit(solution)/shard_map/all_to_all | solution.py:67
  104.0 3.5 %convolution_convert_fusion.3 = bf16[8,128,512]{2,1,0:T(8,128)(2,1)} fusion(bf16[8,128,1024]{2,1,0:T(8,128)(2,1)S(1)} %all_to_all.20, bf16[2,1024,512]{2,1,0:T(8,128)(2,1)} %param.14), kind=kOutput, calls=%fused_computation.34 | convolution fusion | flops 1074266112 | bytes 4194304 | tf_op jit(solution)/shard_map/scd,df->scf/dot_general | solution.py:12
  107.4 1.7 copy.39
  110.5 40.7 %all-to-all-done = bf16[8,128,1024]{2,1,0:T(8,128)(2,1)} async-done(((bf16[8,128,1024]{2,1,0:T(8,128)(2,1)}), bf16[8,128,1024]{2,1,0:T(8,128)(2,1)}, u32[]{:S(2)}, u32[]{:S(2)}) %all-to-all-start) | async-done | bytes 2097184 | tf_op jit(solution)/shard_map/all_to_all | solution.py:67
  151.1 3.1 convolution_convert_fusion.4
  159.1 5.8 %collective-permute-done.3 = bf16[8,128,128]{2,1,0:T(8,128)(2,1)S(1)} collective-permute-done((bf16[8,128,128]{2,1,0:T(8,128)(2,1)S(1)}, bf16[8,128,128]{2,1,0:T(8,128)(2,1)S(1)}, u32[]{:S(2)}, u32[]{:S(2)}) %collective-permute-start.3) | collective-permute-done | bytes 262176 | tf_op jit(solution)/shard_map/ppermute | solution.py:25
  164.9 5.8 %collective-permute-done.4 = bf16[8,128,128]{2,1,0:T(8,128)(2,1)S(1)} collective-permute-done((bf16[8,128,128]{2,1,0:T(8,128)(2,1)S(1)}, bf16[8,128,128]{2,1,0:T(8,128)(2,1)S(1)}, u32[]{:S(2)}, u32[]{:S(2)}) %collective-permute-start.4) | collective-permute-done | bytes 262176 | tf_op jit(solution)/shard_map/ppermute | solution.py:25
  170.7 3.3 %convolution_convert_fusion.5 = bf16[8,128,512]{2,1,0:T(8,128)(2,1)S(1)} fusion(bf16[8,128,1024]{2,1,0:T(8,128)(2,1)} %all-to-all-done, bf16[2,1024,512]{2,1,0:T(8,128)(2,1)} %param.14), kind=kOutput, calls=%fused_computation.36 | convolution fusion | flops 1074266112 | bytes 4194304 | tf_op jit(solution)/shard_map/scd,df->scf/dot_general | solution.py:12
  176.0 5.8 %collective-permute-done.5 = bf16[8,128,128]{2,1,0:T(8,128)(2,1)S(1)} collective-permute-done((bf16[8,128,128]{2,1,0:T(8,128)(2,1)S(1)}, bf16[8,128,128]{2,1,0:T(8,128)(2,1)S(1)}, u32[]{:S(2)}, u32[]{:S(2)}) %collective-permute-start.5) | collective-permute-done | bytes 262176 | tf_op jit(solution)/shard_map/ppermute | solution.py:25
  181.8 4.5 %convolution_convert_fusion = bf16[8,128,1024]{2,1,0:T(8,128)(2,1)} fusion(s32[]{:T(128)S(6)} %select_n.44, bf16[8,128,128]{2,1,0:T(8,128)(2,1)S(1)} %collective-permute-done.5, bf16[8,128,128]{2,1,0:T(8,128)(2,1)S(1)} %collective-permute-done.4, bf16[8,128,128]{2,1,0:T(8,128)(2,1)S(1)} %collective-permute-done.3, bf16[8,128,128]{2,1,0:T(8,128)(2,1)S(1)} %fusion.41, ...), kind=kOutput, calls=%fused_computation.31 | convolution fusion | flops 1083179008 | bytes 4194308 | tf_op jit(solution)/shard_map/scf,fd->scd/dot_general | solution.py:29
  186.3 3.6 %all-to-all-start.3 = ((bf16[8,128,1024]{2,1,0:T(8,128)(2,1)}), bf16[8,128,1024]{2,1,0:T(8,128)(2,1)S(1)}, u32[]{:S(2)}, u32[]{:S(2)}) async-start(bf16[8,128,1024]{2,1,0:T(8,128)(2,1)} %convolution_convert_fusion), calls=%async_computation.3 | async-start | bytes 4194304 | tf_op jit(solution)/shard_map/all_to_all | solution.py:35
  191.2 18.4 %reduce-scatter.13.cloned.1.call-done = bf16[128,1024]{1,0:T(8,128)(2,1)} async-done(((bf16[512,1024]{1,0:T(8,128)(2,1)}), bf16[128,1024]{1,0:T(8,128)(2,1)}) %reduce-scatter.13.cloned.1.call-update) | async-done | bytes 262160
  211.1 5.8 %collective-permute-done = bf16[8,128,128]{2,1,0:T(8,128)(2,1)S(1)} collective-permute-done((bf16[8,128,128]{2,1,0:T(8,128)(2,1)S(1)}, bf16[8,128,128]{2,1,0:T(8,128)(2,1)S(1)}, u32[]{:S(2)}, u32[]{:S(2)}) %collective-permute-start) | collective-permute-done | bytes 262176 | tf_op jit(solution)/shard_map/ppermute | solution.py:25
  216.9 5.8 %collective-permute-done.1 = bf16[8,128,128]{2,1,0:T(8,128)(2,1)S(1)} collective-permute-done((bf16[8,128,128]{2,1,0:T(8,128)(2,1)S(1)}, bf16[8,128,128]{2,1,0:T(8,128)(2,1)S(1)}, u32[]{:S(2)}, u32[]{:S(2)}) %collective-permute-start.1) | collective-permute-done | bytes 262176 | tf_op jit(solution)/shard_map/ppermute | solution.py:25
  222.7 5.8 %collective-permute-done.2 = bf16[8,128,128]{2,1,0:T(8,128)(2,1)S(1)} collective-permute-done((bf16[8,128,128]{2,1,0:T(8,128)(2,1)S(1)}, bf16[8,128,128]{2,1,0:T(8,128)(2,1)S(1)}, u32[]{:S(2)}, u32[]{:S(2)}) %collective-permute-start.2) | collective-permute-done | bytes 262176 | tf_op jit(solution)/shard_map/ppermute | solution.py:25
  228.5 4.4 %convolution_convert_fusion.1 = bf16[8,128,1024]{2,1,0:T(8,128)(2,1)} fusion(s32[]{:T(128)S(6)} %select_n.44, bf16[8,128,128]{2,1,0:T(8,128)(2,1)S(1)} %collective-permute-done.2, bf16[8,128,128]{2,1,0:T(8,128)(2,1)S(1)} %collective-permute-done.1, bf16[8,128,128]{2,1,0:T(8,128)(2,1)S(1)} %collective-permute-done, bf16[8,128,128]{2,1,0:T(8,128)(2,1)S(1)} %fusion.42, ...), kind=kOutput, calls=%fused_computation.32 | convolution fusion | flops 1083179008 | bytes 4194308 | tf_op jit(solution)/shard_map/scf,fd->scd/dot_general | solution.py:29
  232.9 3.9 %all-to-all-done.3 = bf16[8,128,1024]{2,1,0:T(8,128)(2,1)S(1)} async-done(((bf16[8,128,1024]{2,1,0:T(8,128)(2,1)}), bf16[8,128,1024]{2,1,0:T(8,128)(2,1)S(1)}, u32[]{:S(2)}, u32[]{:S(2)}) %all-to-all-start.3) | async-done | bytes 2097184 | tf_op jit(solution)/shard_map/all_to_all | solution.py:35
  236.8 4.3 %all-to-all-start.1 = ((bf16[8,128,1024]{2,1,0:T(8,128)(2,1)}), bf16[8,128,1024]{2,1,0:T(8,128)(2,1)}, u32[]{:S(2)}, u32[]{:S(2)}) async-start(bf16[8,128,1024]{2,1,0:T(8,128)(2,1)} %convolution_convert_fusion.1), calls=%async_computation.1 | async-start | bytes 4194304 | tf_op jit(solution)/shard_map/all_to_all | solution.py:35
  241.5 47.5 %all-to-all-done.1 = bf16[8,128,1024]{2,1,0:T(8,128)(2,1)} async-done(((bf16[8,128,1024]{2,1,0:T(8,128)(2,1)}), bf16[8,128,1024]{2,1,0:T(8,128)(2,1)}, u32[]{:S(2)}, u32[]{:S(2)}) %all-to-all-start.1) | async-done | bytes 2097184 | tf_op jit(solution)/shard_map/all_to_all | solution.py:35
  289.0 2.0 pad_maximum_fusion
  290.9 2.4 copy.34
  293.3 5.5 %gather_fusion.2 = bf16[512,1024]{1,0:T(8,128)(2,1)S(1)} fusion(bf16[2048,1024]{1,0:T(8,128)(2,1)} %bitcast.99, s32[1024]{0:T(1024)S(1)} %get-tuple-element.14), kind=kCustom, calls=%fused_computation.2 | custom fusion | bytes 2099200 | tf_op jit(solution)/shard_map/gather | solution.py:75
  298.8 5.5 %gather_fusion.1 = bf16[512,1024]{1,0:T(8,128)(2,1)S(1)} fusion(bf16[2048,1024]{1,0:T(8,128)(2,1)} %bitcast.100, s32[1024]{0:T(1024)S(1)} %get-tuple-element.15), kind=kCustom, calls=%fused_computation.1 | custom fusion | bytes 2099200 | tf_op jit(solution)/shard_map/gather | solution.py:75
  304.9 5.7 %psum.15 = f32[512]{0:T(512)S(1)} all-reduce(f32[512]{0:T(512)S(1)} %multiply_reduce_fusion), channel_id=1, replica_groups=mesh['ep'=8,'tp'=4] {'tp'}, use_global_device_ids=true, to_apply=%region_11.13 | all-reduce | flops 512 | bytes 4096 | tf_op jit(solution)/shard_map/psum | solution.py:78
  (70 shorter events, 18.7 us)
Async XLA Ops:
  6.5 21.0 %copy-start = (bf16[512,1024]{1,0:T(8,128)(2,1)S(1)}, bf16[512,1024]{1,0:T(8,128)(2,1)}, u32[]{:S(2)}) copy-start(bf16[512,1024]{1,0:T(8,128)(2,1)} %param.10) | copy-start | bytes 3145732
  6.5 21.0 %copy-start.1 = (f32[1024]{0:T(1024)S(1)}, f32[1024]{0:T(1024)}, u32[]{:S(2)}) copy-start(f32[1024]{0:T(1024)} %param.13) | copy-start | bytes 12292
  6.5 149.8 %reduce-scatter.19.cloned.1.call-start = ((), (), s32[]{:S(2)}) async-start(), calls=%async_computation.11 | async-start | bytes 1310720
  41.6 52.7 %copy-start.4 = (bf16[2,1024,512]{2,1,0:T(8,128)(2,1)S(1)}, bf16[2,1024,512]{2,1,0:T(8,128)(2,1)}, u32[]{:S(2)}) copy-start(bf16[2,1024,512]{2,1,0:T(8,128)(2,1)} %param.15) | copy-start | bytes 6291460
  99.5 51.6 %all-to-all-start = ((bf16[8,128,1024]{2,1,0:T(8,128)(2,1)}), bf16[8,128,1024]{2,1,0:T(8,128)(2,1)}, u32[]{:S(2)}, u32[]{:S(2)}) async-start(bf16[8,128,1024]{2,1,0:T(8,128)(2,1)} %get-tuple-element.8), calls=%async_computation | async-start | bytes 4194304 | tf_op jit(solution)/shard_map/all_to_all | solution.py:67
  103.9 53.7 %reduce-scatter.17.cloned.1.call-start = ((), (), s32[]{:S(2)}) async-start(), calls=%async_computation.10 | async-start | bytes 1310720
  110.4 79.5 %reduce-scatter.15.cloned.1.call-start = ((), (), s32[]{:S(2)}) async-start(), calls=%async_computation.9 | async-start | bytes 1310720
  156.3 53.3 %reduce-scatter.13.cloned.1.call-start = ((), (), s32[]{:S(2)}) async-start(), calls=%async_computation.8 | async-start | bytes 1310720
  159.0 5.8 %collective-permute-start.3 = (bf16[8,128,128]{2,1,0:T(8,128)(2,1)S(1)}, bf16[8,128,128]{2,1,0:T(8,128)(2,1)S(1)}, u32[]{:S(2)}, u32[]{:S(2)}) collective-permute-start(bf16[8,128,128]{2,1,0:T(8,128)(2,1)S(1)} %fusion.41), channel_id=1, source_target_pairs={{0,1},{1,2},{2,3},{3,0},{4,5},{5,6},{6,7},{7,4},{8,9},{9,10},{10,1... | collective-permute-start | bytes 786440 | tf_op jit(solution)/shard_map/ppermute | solution.py:25
  164.9 5.8 %collective-permute-start.4 = (bf16[8,128,128]{2,1,0:T(8,128)(2,1)S(1)}, bf16[8,128,128]{2,1,0:T(8,128)(2,1)S(1)}, u32[]{:S(2)}, u32[]{:S(2)}) collective-permute-start(bf16[8,128,128]{2,1,0:T(8,128)(2,1)S(1)} %collective-permute-done.3), channel_id=1, source_target_pairs={{0,1},{1,2},{2,3},{3,0},{4,5},{5,6},{6,7},{7,4},{8,9},{9,10},{10,1... | collective-permute-start | bytes 786440 | tf_op jit(solution)/shard_map/ppermute | solution.py:25
  170.7 11.2 %collective-permute-start.5 = (bf16[8,128,128]{2,1,0:T(8,128)(2,1)S(1)}, bf16[8,128,128]{2,1,0:T(8,128)(2,1)S(1)}, u32[]{:S(2)}, u32[]{:S(2)}) collective-permute-start(bf16[8,128,128]{2,1,0:T(8,128)(2,1)S(1)} %collective-permute-done.4), channel_id=1, source_target_pairs={{0,1},{1,2},{2,3},{3,0},{4,5},{5,6},{6,7},{7,4},{8,9},{9,10},{10,1... | collective-permute-start | bytes 786440 | tf_op jit(solution)/shard_map/ppermute | solution.py:25
  186.3 50.5 %all-to-all-start.3 = ((bf16[8,128,1024]{2,1,0:T(8,128)(2,1)}), bf16[8,128,1024]{2,1,0:T(8,128)(2,1)S(1)}, u32[]{:S(2)}, u32[]{:S(2)}) async-start(bf16[8,128,1024]{2,1,0:T(8,128)(2,1)} %convolution_convert_fusion), calls=%async_computation.3 | async-start | bytes 4194304 | tf_op jit(solution)/shard_map/all_to_all | solution.py:35
  211.0 5.8 %collective-permute-start = (bf16[8,128,128]{2,1,0:T(8,128)(2,1)S(1)}, bf16[8,128,128]{2,1,0:T(8,128)(2,1)S(1)}, u32[]{:S(2)}, u32[]{:S(2)}) collective-permute-start(bf16[8,128,128]{2,1,0:T(8,128)(2,1)S(1)} %fusion.42), channel_id=1, source_target_pairs={{0,1},{1,2},{2,3},{3,0},{4,5},{5,6},{6,7},{7,4},{8,9},{9,10},{10,1... | collective-permute-start | bytes 786440 | tf_op jit(solution)/shard_map/ppermute | solution.py:25
  216.9 5.8 %collective-permute-start.1 = (bf16[8,128,128]{2,1,0:T(8,128)(2,1)S(1)}, bf16[8,128,128]{2,1,0:T(8,128)(2,1)S(1)}, u32[]{:S(2)}, u32[]{:S(2)}) collective-permute-start(bf16[8,128,128]{2,1,0:T(8,128)(2,1)S(1)} %collective-permute-done), channel_id=1, source_target_pairs={{0,1},{1,2},{2,3},{3,0},{4,5},{5,6},{6,7},{7,4},{8,9},{9,10},{10,1... | collective-permute-start | bytes 786440 | tf_op jit(solution)/shard_map/ppermute | solution.py:25
  222.7 5.8 %collective-permute-start.2 = (bf16[8,128,128]{2,1,0:T(8,128)(2,1)S(1)}, bf16[8,128,128]{2,1,0:T(8,128)(2,1)S(1)}, u32[]{:S(2)}, u32[]{:S(2)}) collective-permute-start(bf16[8,128,128]{2,1,0:T(8,128)(2,1)S(1)} %collective-permute-done.1), channel_id=1, source_target_pairs={{0,1},{1,2},{2,3},{3,0},{4,5},{5,6},{6,7},{7,4},{8,9},{9,10},{10,1... | collective-permute-start | bytes 786440 | tf_op jit(solution)/shard_map/ppermute | solution.py:25
  232.9 8.6 %copy-start.3 = (f32[512,2]{0,1:T(2,128)S(1)}, f32[512,2]{0,1:T(2,128)}, u32[]{:S(2)}) copy-start(f32[512,2]{0,1:T(2,128)} %param.12) | copy-start | bytes 12292
  236.8 52.2 %all-to-all-start.1 = ((bf16[8,128,1024]{2,1,0:T(8,128)(2,1)}), bf16[8,128,1024]{2,1,0:T(8,128)(2,1)}, u32[]{:S(2)}, u32[]{:S(2)}) async-start(bf16[8,128,1024]{2,1,0:T(8,128)(2,1)} %convolution_convert_fusion.1), calls=%async_computation.1 | async-start | bytes 4194304 | tf_op jit(solution)/shard_map/all_to_all | solution.py:35
  304.2 6.3 %copy-start.2 = (f32[1024]{0:T(1024)S(1)}, f32[1024]{0:T(1024)}, u32[]{:S(2)}) copy-start(f32[1024]{0:T(1024)} %param.17) | copy-start | bytes 12292
Sparse Core Ops, SparseCore 0:
  99.7 23.8 reduce-scatter.18
  126.1 24.8 reduce-scatter.16
  156.4 26.7 reduce-scatter.14
  185.6 23.9 reduce-scatter.12
